TPU v7x, 128 devices: a whole 4x4x4 slice. The times are simulated.
128 devices in a mesh: sp: 16 (over z, y), dp: 8 (over x, core).
Axes of the slice: x: 4, y: 4, z: 4, core: 2. Of those that a mesh axis runs over, the one named last changes fastest.
Arguments:
- query: bfloat16 [8, 3072, 3072], P('dp', 'sp'), may hold values from -18 to 18
- latent: bfloat16 [8, 3072, 1024], P('dp', 'sp'), may hold values from -6 to 6
- rope_key: bfloat16 [8, 3072, 32], P('dp', 'sp'), may hold values from -5 to 5
- latent_norm_gain: float32 [1024], replicated, may hold values from 0.1 to 1.9
- key_up_matrix: bfloat16 [2048, 1024], P('dp'), may hold values from -0.1875 to 0.1875
- value_up_matrix: bfloat16 [2048, 1024], P('dp'), may hold values from -0.1875 to 0.1875
- out_grad: bfloat16 [8, 3072, 2048], P('dp', 'sp'), may hold values from -6 to 6
Outputs:
- query_grad: bfloat16 [8, 3072, 3072], P('dp', 'sp')
- latent_grad: float32 [8, 3072, 1024], P('dp', 'sp')
- rope_key_grad: float32 [8, 3072, 32], P('dp', 'sp')
- key_weight_grad: float32 [2048, 1024], P('dp')
- value_weight_grad: float32 [2048, 1024], P('dp')
- gain_grad: float32 [1024], replicated
All inputs are finite; a program needn't handle non-finite values.
Results may differ from a plain program's by a relative error of at most 0.011.
Values may be sent and summed in bfloat16 or wider, within the bound.
A program may use at most 256 MiB of HBM per device.

v0:
```python
import functools
import jax
import jax.numpy as jnp
from jax import lax
from jax.sharding import Mesh
from jax.sharding import PartitionSpec as P

ATTENTION_HEADS = 32
PLAIN_HEAD_WIDTH = 64
ROPE = 32
VALUE_HEAD_WIDTH = 64
SPAN = 64
DP = ("dp_0", "dp_1")
SP = ("sp_0", "sp_1")
SP_DP = ("sp_0", "sp_1", "dp_0", "dp_1")
eps = 1e-06
rope_base = 10000.0


def from_everyone(value, axis):
    size = lax.axis_size(axis)
    return lax.all_to_all(
        jnp.broadcast_to(value[None], (size, *value.shape)), axis, 0, 0, tiled=True
    )


def in_order(blocks, dim):
    blocks = jnp.moveaxis(blocks, 0, dim)
    shape = blocks.shape
    return blocks.reshape(*shape[:dim], shape[dim] * shape[dim + 1], *shape[dim + 2 :])


def gather_directly(value, axis, dim):
    blocks = from_everyone(value, axis)
    return in_order(blocks, dim)


def split_up(value, dim, size):
    shape = value.shape
    blocks = value.reshape(*shape[:dim], size, shape[dim] // size, *shape[dim + 1 :])
    return jnp.moveaxis(blocks, dim, 0)


def sent_and_summed(value, axis, dim):
    blocks = split_up(value, dim, lax.axis_size(axis))
    arrived = lax.all_to_all(blocks, axis, split_axis=0, concat_axis=0, tiled=True)
    return arrived.sum(axis=0)


def edges_of(length, count):
    unit = 8 if length >= 8 * count else 1
    return [length // unit * k // count * unit for k in range(1, count)]


def all_blocks(value, axes, turns):
    blocks = value[None]
    for k in turns:
        blocks = lax.all_gather(blocks, axes[k], axis=0, tiled=True)
    carried = [lax.axis_size(axes[k]) for k in reversed(turns)]
    blocks = blocks.reshape(*carried, *value.shape)
    turned = sorted(range(len(turns)), key=lambda place: turns[len(turns) - 1 - place])
    return blocks.transpose(*turned, *range(len(turns), blocks.ndim)).reshape(-1, *value.shape)


def gather_all_axes(value, axes, dim):
    numbers = list(range(len(axes)))[::-1]
    widest = value.shape.index(max(value.shape[:-1] or value.shape))
    edges = [0, *edges_of(value.shape[widest], len(axes)), value.shape[widest]]
    finished = []
    for k, (start, end) in enumerate(zip(edges, edges[1:])):
        if end > start:
            section = lax.slice_in_dim(value, start, end, axis=widest)
            finished.append(all_blocks(section, axes, numbers[k:] + numbers[:k]))
    return in_order(jnp.concatenate(finished, axis=widest + 1), dim)


def by_axis(value, axes):
    return functools.reduce(lax.psum, axes, value)


def rotate(values, cosine, sine):
    half = values.shape[-1] // 2
    first = values[..., :half]
    second = values[..., half:]
    return jnp.concatenate(
        [first * cosine - second * sine, second * cosine + first * sine], axis=-1
    )


def angles(length, width):
    inverse = 1.0 / rope_base ** (jnp.arange(0, width, 2, dtype=jnp.float32) / width)
    turned = jnp.arange(length, dtype=jnp.float32)[:, None] * inverse[None, :]
    return (jnp.cos(turned), jnp.sin(turned))


def attend_backward(arrived, rope_full):
    f32 = jnp.float32
    bf16 = jnp.bfloat16
    length = arrived.shape[0]
    local_heads = arrived.shape[1]
    width = PLAIN_HEAD_WIDTH + ROPE
    scale = width ** (-0.5)
    block = 512
    cosine, sine = angles(length, ROPE)
    neg = jnp.finfo(f32).min
    q_nope = arrived[:, :, :PLAIN_HEAD_WIDTH]
    q_rope = rotate(
        arrived[:, :, PLAIN_HEAD_WIDTH:width].astype(f32), cosine[:, None, :], sine[:, None, :]
    ).astype(bf16)
    key_nope = arrived[:, :, width : width + PLAIN_HEAD_WIDTH]
    values = arrived[:, :, width + PLAIN_HEAD_WIDTH : width + PLAIN_HEAD_WIDTH + VALUE_HEAD_WIDTH]
    d_out = arrived[:, :, width + PLAIN_HEAD_WIDTH + VALUE_HEAD_WIDTH :]
    k_rope = rotate(rope_full.astype(f32), cosine, sine).astype(bf16)
    dk_nope = jnp.zeros((length, local_heads, PLAIN_HEAD_WIDTH), f32)
    dk_rope = jnp.zeros((length, ROPE), f32)
    d_vals = jnp.zeros((length, local_heads, VALUE_HEAD_WIDTH), f32)
    dq_parts = []
    for begin in range(0, length, block):
        end = begin + block
        qn = q_nope[begin:end]
        qr = q_rope[begin:end]
        go = d_out[begin:end]
        scores = jnp.einsum("qhd,khd->hqk", qn, key_nope[:end], preferred_element_type=f32)
        scores = (
            scores + jnp.einsum("qhd,kd->hqk", qr, k_rope[:end], preferred_element_type=f32)
        ) * scale
        q_seg = jnp.arange(begin, end) // SPAN
        k_seg = jnp.arange(end) // SPAN
        allowed = k_seg[None, :] <= q_seg[:, None]
        scores = jnp.where(allowed[None], scores, neg)
        probs = jax.nn.softmax(scores, axis=-1)
        d_probs = jnp.einsum("qhd,khd->hqk", go, values[:end], preferred_element_type=f32)
        d_scores = probs * (d_probs - jnp.sum(probs * d_probs, axis=-1, keepdims=True))
        ds_b = d_scores.astype(bf16)
        p_b = probs.astype(bf16)
        dq_n = jnp.einsum("hqk,khd->qhd", ds_b, key_nope[:end], preferred_element_type=f32) * scale
        dq_r = jnp.einsum("hqk,kd->qhd", ds_b, k_rope[:end], preferred_element_type=f32) * scale
        dq_r = rotate(dq_r, cosine[begin:end, None, :], -sine[begin:end, None, :])
        dq_parts.append(jnp.concatenate([dq_n, dq_r], axis=-1).astype(bf16))
        dk_nope = dk_nope.at[:end].add(
            jnp.einsum("hqk,qhd->khd", ds_b, qn, preferred_element_type=f32) * scale
        )
        dk_rope = dk_rope.at[:end].add(
            jnp.einsum("hqk,qhd->kd", ds_b, qr, preferred_element_type=f32) * scale
        )
        d_vals = d_vals.at[:end].add(
            jnp.einsum("hqk,qhd->khd", p_b, go, preferred_element_type=f32)
        )
    query_part = jnp.concatenate(dq_parts, axis=0)
    grads = jnp.concatenate([query_part, dk_nope.astype(bf16), d_vals.astype(bf16)], axis=-1)
    return (grads, rotate(dk_rope, cosine, -sine))


def local(query, latent, rope_key, latent_norm_gain, key_up_matrix, value_up_matrix, out_grad):
    f32 = jnp.float32
    bf16 = jnp.bfloat16
    tokens = latent.shape[1]
    width = PLAIN_HEAD_WIDTH + ROPE
    head_cols = ATTENTION_HEADS * PLAIN_HEAD_WIDTH
    lat = latent[0].astype(f32)
    inv_rms = lax.rsqrt(jnp.mean(lat * lat, axis=-1, keepdims=True) + eps)
    normed = lat * inv_rms
    nlat = (normed * latent_norm_gain).astype(bf16)
    stacked = jnp.stack([key_up_matrix, value_up_matrix])
    whole = lax.all_gather(stacked, DP, axis=1, tiled=True)
    kv_tok = jnp.einsum("tc,gnc->tgn", nlat, whole, preferred_element_type=f32).astype(bf16)
    heads_query = query[0].reshape(tokens, ATTENTION_HEADS, width)
    key_nope = kv_tok[:, 0].reshape(tokens, ATTENTION_HEADS, PLAIN_HEAD_WIDTH)
    values = kv_tok[:, 1].reshape(tokens, ATTENTION_HEADS, VALUE_HEAD_WIDTH)
    d_out = out_grad[0].reshape(tokens, ATTENTION_HEADS, VALUE_HEAD_WIDTH)
    packed = jnp.concatenate([heads_query, key_nope, values, d_out], axis=2)
    arrived = lax.all_to_all(packed, SP, split_axis=1, concat_axis=0, tiled=True)
    rope_full = gather_directly(rope_key[0], SP, 0)
    grads_heads, rope_full_grad = attend_backward(arrived, rope_full)
    returned = lax.all_to_all(grads_heads, SP, split_axis=0, concat_axis=1, tiled=True)
    rope_grad = sent_and_summed(rope_full_grad, SP, 0)
    query_grad = returned[:, :, :width].reshape(tokens, ATTENTION_HEADS * width)
    key_cols = returned[:, :, width : width + PLAIN_HEAD_WIDTH].reshape(tokens, head_cols)
    value_cols = returned[:, :, width + PLAIN_HEAD_WIDTH :].reshape(tokens, head_cols)
    dkv = jnp.stack([key_cols, value_cols], axis=1)
    d_nlat = jnp.einsum("tgn,gnc->tc", dkv, whole, preferred_element_type=f32)
    latents_all = gather_all_axes(nlat[None], DP, 0)
    columns = lax.all_to_all(dkv[None], DP, split_axis=3, concat_axis=0, tiled=True)
    partial_value = jnp.einsum("stgr,stc->grc", columns, latents_all, preferred_element_type=f32)
    weight_grads = lax.psum(partial_value, SP)
    gain_grad = by_axis(jnp.sum(d_nlat * normed, axis=0), SP_DP)
    scaled = d_nlat * latent_norm_gain
    latent_grad = inv_rms * (scaled - normed * jnp.mean(scaled * normed, axis=-1, keepdims=True))
    return (
        query_grad[None],
        latent_grad[None],
        rope_grad[None],
        weight_grads[0],
        weight_grads[1],
        gain_grad,
    )


def solution(mesh):
    split = Mesh(mesh.devices.reshape(4, 4, 4, 2), ("sp_0", "sp_1", "dp_0", "dp_1"))
    in_specs = (
        P(DP, SP, None),
        P(DP, SP, None),
        P(DP, SP, None),
        P(),
        P(DP, None),
        P(DP, None),
        P(DP, SP, None),
    )
    out_specs = (P(DP, SP, None), P(DP, SP, None), P(DP, SP, None), P(DP, None), P(DP, None), P())
    return jax.shard_map(local, mesh=split, in_specs=in_specs, out_specs=out_specs, check_vma=False)
```

profile of v0, /device:TPU:0, one launch (start us, length us, event | category | flops | bytes accessed | tf_op | source)
XLA Modules:
  0.0 623.8 jit_solution(4799579515403184759)
XLA Ops:
  11.1 14.5 %all-gather.2 = bf16[4,96,1024]{2,1,0:T(8,128)(2,1)} all-gather(bf16[1,96,1024]{2,1,0:T(8,128)(2,1)S(1)} %get-tuple-element.261), channel_id=4, replica_groups=mesh['sp_0'=4,'sp_1'=4,'dp_0'=4,'dp_1'=2] {'dp_0'}, dimensions={0}, use_global_device_ids=true | all-gather | bytes 983040 | tf_op jit(solution)/shard_map/all_gather | solution.py:58
  26.4 8.6 %all-to-all-start.1 = ((bf16[16,192,32]{1,2,0:T(8,128)(2,1)}), bf16[16,192,32]{1,2,0:T(8,128)(2,1)S(1)}, u32[]{:S(2)}, u32[]{:S(2)}) async-start(bf16[16,192,32]{1,2,0:T(8,128)(2,1)} %broadcast_in_dim.80), calls=%async_computation.1 | async-start | bytes 524288 | tf_op jit(solution)/shard_map/all_to_all | solution.py:22
  45.3 17.1 %all-gather.8.cloned.1.call-done = bf16[2,2048,1024]{2,1,0:T(8,128)(2,1)} async-done(((bf16[2,256,1024]{2,1,0:T(8,128)(2,1)}), bf16[2,2048,1024]{2,1,0:T(8,128)(2,1)}) %all-gather.8.cloned.1.call-update) | async-done | bytes 8388624 | tf_op jit(solution)/shard_map/all_gather | solution.py:165
  88.3 7.2 %all-to-all-start = ((bf16[192,32,288]{2,0,1:T(8,128)(2,1)}), bf16[192,32,288]{2,0,1:T(8,128)(2,1)}, u32[]{:S(2)}, u32[]{:S(2)}) async-start(bf16[192,32,288]{2,0,1:T(8,128)(2,1)} %copy.83), calls=%async_computation | async-start | bytes 9437184 | tf_op jit(solution)/shard_map/all_to_all | solution.py:172
  105.9 61.1 %all-to-all-done = bf16[192,32,288]{2,0,1:T(8,128)(2,1)} async-done(((bf16[192,32,288]{2,0,1:T(8,128)(2,1)}), bf16[192,32,288]{2,0,1:T(8,128)(2,1)}, u32[]{:S(2)}, u32[]{:S(2)}) %all-to-all-start) | async-done | bytes 3538976 | tf_op jit(solution)/shard_map/all_to_all | solution.py:172
  167.0 8.3 %copy.84 = bf16[16,192,2,288]{1,0,3,2:T(8,128)(2,1)} copy(bf16[16,192,2,288]{3,1,2,0:T(8,128)(2,1)} %bitcast.8) | data formatting | bytes 7077888 | tf_op jit(solution)/shard_map/all_to_all | solution.py:172
  175.3 7.2 %all_to_all.48 = bf16[3072,2,288]{0,2,1:T(8,128)(2,1)S(1)} reshape(bf16[16,192,2,288]{1,0,3,2:T(8,128)(2,1)} %copy.84) | data formatting | bytes 7077888 | tf_op jit(solution)/shard_map/all_to_all | solution.py:172
  225.4 7.3 %fusion.297 = (f32[2,512]{1,0:T(2,128)S(1)}, f32[2,512,2048]{2,1,0:T(8,128)S(1)}) fusion(f32[2,512,2048]{2,1,0:T(8,128)} %fusion.11), kind=kOutput, calls=%fused_computation.433 | output fusion | flops 4196351 | bytes 16781312 | tf_op jit(solution)/shard_map/sub | solution.py:131
  282.7 14.9 %fusion.299 = (f32[2,512]{1,0:T(2,128)S(1)}, f32[2,512,3072]{2,1,0:T(8,128)}) fusion(f32[2,512,3072]{2,1,0:T(8,128)} %fusion.7), kind=kOutput, calls=%fused_computation.435 | output fusion | flops 6294527 | bytes 25169920 | tf_op jit(solution)/shard_map/sub | solution.py:131
  297.6 11.8 %multiply_reduce_fusion = (f32[2,512]{1,0:T(2,128)S(1)}, f32[2,512,3072]{2,1,0:T(8,128)}) fusion(f32[2,512,3072]{2,1,0:T(8,128)} %get-tuple-element.301, f32[2,512]{1,0:T(2,128)S(1)} %get-tuple-element.300, bf16[3072,2,288]{0,2,1:T(8,128)(2,1)} %copy-done.6), kind=kOutput, calls=%fused_computation.10 | convolution fusion | flops 412089344 | bytes 26091520 | tf_op jit(solution)/shard_map/qhd,khd->hqk/dot_general | solution.py:132
  309.5 7.4 %multiply_convert_fusion = bf16[2,512,3072]{2,1,0:T(8,128)(2,1)S(1)} fusion(f32[2,512,3072]{2,1,0:T(8,128)} %get-tuple-element.313, f32[2,512]{1,0:T(2,128)S(1)} %get-tuple-element.312, f32[2,512,3072]{2,1,0:T(8,128)S(1)} %bitcast.325, f32[2,512]{1,0:T(2,128)S(1)} %get-tuple-element.300), kind=kLoop, calls=%fused_computation.9 | loop fusion | flops 12582912 | bytes 31465472 | tf_op jit(solution)/shard_map/convert_element_type | solution.py:134
  325.9 6.4 %fusion.99 = f32[3072,2,64]{0,2,1:T(8,128)} fusion(f32[3072,2,64]{0,2,1:T(8,128)} %scatter-add.59, f32[512,2,64]{0,2,1:T(8,128)} %convolution_bitcast_fusion.5, bf16[3072,2,288]{0,2,1:T(8,128)(2,1)} %copy-done.6, f32[2,512]{1,0:T(2,128)S(1)} %get-tuple-element.292, f32[2,512,1024]{2,1,0:T(8,128)} %copy-done.19), kind=kOutput, calls=%fused_computation.121 | convolution fusion | flops 137496576 | bytes 9310208 | tf_op jit(solution)/shard_map/hqk,qhd->khd/dot_general | solution.py:147
  335.3 8.0 %fusion.77 = f32[3072,2,64]{0,2,1:T(8,128)} fusion(f32[3072,2,64]{0,2,1:T(8,128)} %fusion.99, bf16[3072,2,288]{0,2,1:T(8,128)(2,1)} %copy-done.6, f32[2,512]{1,0:T(2,128)S(1)} %get-tuple-element.294, f32[2,512,1536]{2,1,0:T(8,128)} %copy-done.16), kind=kOutput, calls=%fused_computation.91 | convolution fusion | flops 206244352 | bytes 14290944 | tf_op jit(solution)/shard_map/hqk,qhd->khd/dot_general | solution.py:147
  346.1 9.4 %fusion.65 = f32[3072,2,64]{0,2,1:T(8,128)} fusion(f32[3072,2,64]{0,2,1:T(8,128)} %fusion.77, bf16[3072,2,288]{0,2,1:T(8,128)(2,1)} %copy-done.6, f32[2,512]{1,0:T(2,128)S(1)} %get-tuple-element.296, f32[2,512,2048]{2,1,0:T(8,128)} %fusion.11), kind=kOutput, calls=%fused_computation.84 | convolution fusion | flops 274992128 | bytes 19009536 | tf_op jit(solution)/shard_map/hqk,qhd->khd/dot_general | solution.py:147
  359.9 11.3 %fusion.31 = f32[3072,2,64]{0,2,1:T(8,128)} fusion(f32[3072,2,64]{0,2,1:T(8,128)} %fusion.65, bf16[3072,2,288]{0,2,1:T(8,128)(2,1)} %copy-done.6, f32[2,512]{1,0:T(2,128)S(1)} %get-tuple-element.298, f32[2,512,2560]{2,1,0:T(8,128)} %copy-done.3), kind=kOutput, calls=%fused_computation.52 | convolution fusion | flops 343739904 | bytes 23728128 | tf_op jit(solution)/shard_map/hqk,qhd->khd/dot_general | solution.py:147
  376.3 12.7 %fusion.42 = bf16[3072,2,64]{0,2,1:T(8,128)(2,1)} fusion(f32[3072,2,64]{0,2,1:T(8,128)} %fusion.31, bf16[3072,2,288]{0,2,1:T(8,128)(2,1)} %copy-done.6, f32[2,512]{1,0:T(2,128)S(1)} %copy-done.72, f32[2,512,3072]{2,1,0:T(8,128)} %fusion.7), kind=kOutput, calls=%fused_computation.58 | convolution fusion | flops 412880896 | bytes 27660288 | tf_op jit(solution)/shard_map/hqk,qhd->khd/dot_general | solution.py:147
  396.7 8.6 %copy.95 = bf16[3072,2,224]{2,1,0:T(2,128)(2,1)} copy(bf16[3072,2,224]{0,2,1:T(8,128)(2,1)} %pad_maximum_fusion.1) | data formatting | bytes 5505024 | tf_op jit(solution)/shard_map/concatenate | solution.py:150
  424.4 31.9 %all-to-all-done.2 = bf16[3072,2,224]{2,1,0:T(2,128)(2,1)} async-done(((bf16[3072,2,224]{2,1,0:T(2,128)(2,1)}), bf16[3072,2,224]{2,1,0:T(2,128)(2,1)}, u32[]{:S(2)}, u32[]{:S(2)}) %all-to-all-start.2) | async-done | bytes 2752544 | tf_op jit(solution)/shard_map/all_to_all | solution.py:175
  498.8 14.3 %all-to-all-done.4 = bf16[1,192,2,2048]{1,2,0,3:T(2,128)(2,1)} async-done(((bf16[1,192,2,2048]{1,2,0,3:T(2,128)(2,1)}), bf16[1,192,2,2048]{1,2,0,3:T(2,128)(2,1)}, u32[]{:S(2)}, u32[]{:S(2)}) %all-to-all-start.4) | async-done | bytes 1572896 | tf_op jit(solution)/shard_map/all_to_all | solution.py:183
  524.9 19.4 %all_to_all.64 = f32[16,192,32]{1,2,0:T(8,128)} all-to-all(f32[16,192,32]{1,2,0:T(8,128)S(1)} %copy.104), channel_id=1, replica_groups=mesh['sp_0'=4,'sp_1'=4,'dp_0'=4,'dp_1'=2] {'sp_0','sp_1'}, dimensions={0} | all-to-all | bytes 786432 | tf_op jit(solution)/shard_map/all_to_all | solution.py:46
  555.6 8.8 %psum.36 = f32[1024]{0:T(1024)S(1)} all-reduce(f32[1024]{0:T(1024)S(1)} %get-tuple-element.246), channel_id=1, replica_groups=mesh['sp_0'=4,'sp_1'=4,'dp_0'=4,'dp_1'=2] {'sp_0'}, use_global_device_ids=true, to_apply=%region_23.24 | all-reduce | flops 1024 | bytes 8192 | tf_op jit(solution)/shard_map/psum | solution.py:78
  564.4 8.7 %psum.37 = f32[1024]{0:T(1024)S(1)} all-reduce(f32[1024]{0:T(1024)S(1)} %psum.36), channel_id=1, replica_groups=mesh['sp_0'=4,'sp_1'=4,'dp_0'=4,'dp_1'=2] {'sp_1'}, use_global_device_ids=true, to_apply=%region_24.25 | all-reduce | flops 1024 | bytes 8192 | tf_op jit(solution)/shard_map/psum | solution.py:78
  573.2 9.4 %psum.38 = f32[1024]{0:T(1024)S(1)} all-reduce(f32[1024]{0:T(1024)S(1)} %psum.37), channel_id=1, replica_groups=mesh['sp_0'=4,'sp_1'=4,'dp_0'=4,'dp_1'=2] {'dp_0'}, use_global_device_ids=true, to_apply=%region_25.26 | all-reduce | flops 1024 | bytes 8192 | tf_op jit(solution)/shard_map/psum | solution.py:78
  586.8 27.2 %all-reduce.5.cloned.1.call-done = f32[2,256,1024]{2,1,0:T(8,128)} async-done(((f32[2,256,1024]{2,1,0:T(8,128)}), f32[2,256,1024]{2,1,0:T(8,128)}) %all-reduce.5.cloned.1.call-update) | async-done | bytes 2097168 | tf_op jit(solution)/shard_map/psum | solution.py:185
  (322 shorter events, 266.9 us)
Async XLA Ops:
  7.2 18.4 %copy-start.73 = (bf16[1,192,32]{1,2,0:T(8,128)(2,1)S(1)}, bf16[1,192,32]{1,2,0:T(8,128)(2,1)}, u32[]{:S(2)}) copy-start(bf16[1,192,32]{1,2,0:T(8,128)(2,1)} %param.51) | copy-start | bytes 36868
  7.2 55.2 %all-gather.8.cloned.1.call-start = ((), (), s32[]{:S(2)}) async-start(), calls=%async_computation.5 | async-start | bytes 9437184 | tf_op jit(solution)/shard_map/all_gather | solution.py:165
  9.6 28.7 %copy-start.41 = (bf16[1,192,2048]{2,1,0:T(8,128)(2,1)S(1)}, bf16[1,192,2048]{2,1,0:T(8,128)(2,1)}, u32[]{:S(2)}) copy-start(bf16[1,192,2048]{2,1,0:T(8,128)(2,1)} %param.55) | copy-start | bytes 2359300
  9.6 400.9 %all-gather.12.cloned.1.call-start = ((), (), s32[]{:S(2)}) async-start(), calls=%async_computation.8 | async-start | bytes 2359296 | tf_op jit(solution)/shard_map/all_gather | solution.py:58
  10.9 51.5 %copy-start.74 = (f32[192]{0:T(256)}, f32[192]{0:T(256)S(1)}, u32[]{:S(2)}) copy-start(f32[192]{0:T(256)S(1)} %add_rsqrt_fusion) | copy-start | bytes 2308
  26.4 62.0 %all-to-all-start.1 = ((bf16[16,192,32]{1,2,0:T(8,128)(2,1)}), bf16[16,192,32]{1,2,0:T(8,128)(2,1)S(1)}, u32[]{:S(2)}, u32[]{:S(2)}) async-start(bf16[16,192,32]{1,2,0:T(8,128)(2,1)} %broadcast_in_dim.80), calls=%async_computation.1 | async-start | bytes 524288 | tf_op jit(solution)/shard_map/all_to_all | solution.py:22
  35.0 383.5 %all-gather.10.cloned.1.call-start = ((), (), s32[]{:S(2)}) async-start(), calls=%async_computation.7 | async-start | bytes 1966080 | tf_op jit(solution)/shard_map/all_gather | solution.py:58
  88.3 78.7 %all-to-all-start = ((bf16[192,32,288]{2,0,1:T(8,128)(2,1)}), bf16[192,32,288]{2,0,1:T(8,128)(2,1)}, u32[]{:S(2)}, u32[]{:S(2)}) async-start(bf16[192,32,288]{2,0,1:T(8,128)(2,1)} %copy.83), calls=%async_computation | async-start | bytes 9437184 | tf_op jit(solution)/shard_map/all_to_all | solution.py:172
  95.6 8.9 %copy-start.76 = (f32[16]{0:T(128)}, f32[16]{0:T(128)S(1)}, u32[]{:S(2)}) copy-start(f32[16]{0:T(128)S(1)} %negate_power_fusion) | copy-start | bytes 196
  182.5 30.2 %copy-start.6 = (bf16[3072,2,288]{0,2,1:T(8,128)(2,1)}, bf16[3072,2,288]{0,2,1:T(8,128)(2,1)S(1)}, u32[]{:S(2)}) copy-start(bf16[3072,2,288]{0,2,1:T(8,128)(2,1)S(1)} %all_to_all.48) | copy-start | bytes 10616836
  258.5 7.3 %slice-start.7 = ((s8[10485760]{0:T(1024)(128)(4,1)}), s8[2097152]{0:T(1024)(128)(4,1)S(1)}, s32[]{:S(2)}) async-start(s8[10485760]{0:T(1024)(128)(4,1)} %bitcast.326), calls=%async_computation.16 | async-start | bytes 4194304
  297.6 11.8 %copy-start.71 = (f32[2,512]{1,0:T(2,128)}, f32[2,512]{1,0:T(2,128)S(1)}, u32[]{:S(2)}) copy-start(f32[2,512]{1,0:T(2,128)S(1)} %get-tuple-element.300) | copy-start | bytes 12292
  297.6 11.8 %slice-start.2 = ((s8[12582912]{0:T(1024)(128)(4,1)}), s8[4194304]{0:T(1024)(128)(4,1)S(1)}, s32[]{:S(2)}) async-start(s8[12582912]{0:T(1024)(128)(4,1)} %bitcast.324), calls=%async_computation.11 | async-start | bytes 8388608
  297.6 11.8 %slice-start.3 = ((s8[12582912]{0:T(1024)(128)(4,1)}), s8[4194304]{0:T(1024)(128)(4,1)S(1)}, s32[]{:S(2)}) async-start(s8[12582912]{0:T(1024)(128)(4,1)} %bitcast.324), calls=%async_computation.12 | async-start | bytes 8388608
  297.6 11.8 %slice-start.4 = ((s8[12582912]{0:T(1024)(128)(4,1)}), s8[4194304]{0:T(1024)(128)(4,1)S(1)}, s32[]{:S(2)}) async-start(s8[12582912]{0:T(1024)(128)(4,1)} %bitcast.324), calls=%async_computation.13 | async-start | bytes 8388608
  405.3 50.9 %all-to-all-start.2 = ((bf16[3072,2,224]{2,1,0:T(2,128)(2,1)}), bf16[3072,2,224]{2,1,0:T(2,128)(2,1)}, u32[]{:S(2)}, u32[]{:S(2)}) async-start(bf16[3072,2,224]{2,1,0:T(2,128)(2,1)} %copy.95), calls=%async_computation.2 | async-start | bytes 6291456 | tf_op jit(solution)/shard_map/all_to_all | solution.py:175
  414.7 7.3 %copy-start.10 = (bf16[3072,2,16]{0,2,1:T(8,128)(2,1)S(1)}, bf16[3072,2,16]{0,2,1:T(8,128)(2,1)}, u32[]{:S(2)}) copy-start(bf16[3072,2,16]{0,2,1:T(8,128)(2,1)} %copy-done.8) | copy-start | bytes 589828
  414.7 7.3 %copy-start.13 = (bf16[3072,2,16]{0,2,1:T(8,128)(2,1)S(1)}, bf16[3072,2,16]{0,2,1:T(8,128)(2,1)}, u32[]{:S(2)}) copy-start(bf16[3072,2,16]{0,2,1:T(8,128)(2,1)} %copy-done.11) | copy-start | bytes 589828
  481.6 31.5 %all-to-all-start.4 = ((bf16[1,192,2,2048]{1,2,0,3:T(2,128)(2,1)}), bf16[1,192,2,2048]{1,2,0,3:T(2,128)(2,1)}, u32[]{:S(2)}, u32[]{:S(2)}) async-start(bf16[1,192,2,2048]{1,2,0,3:T(2,128)(2,1)} %copy.105), calls=%async_computation.4 | async-start | bytes 4194304 | tf_op jit(solution)/shard_map/all_to_all | solution.py:183
  485.9 128.1 %all-reduce.5.cloned.1.call-start = ((), (), s32[]{:S(2)}) async-start(), calls=%async_computation.6 | async-start | bytes 4194304 | tf_op jit(solution)/shard_map/psum | solution.py:185
  486.0 10.6 %slice-start = ((s8[6291456]{0:T(1024)(128)(4,1)}), s8[4194304]{0:T(1024)(128)(4,1)S(1)}, s32[]{:S(2)}) async-start(s8[6291456]{0:T(1024)(128)(4,1)} %bitcast.322), calls=%async_computation.9 | async-start | bytes 8388608
  488.4 8.2 %slice-start.1 = ((s8[6291456]{0:T(1024)(128)(4,1)}), s8[2097152]{0:T(1024)(128)(4,1)S(1)}, s32[]{:S(2)}) async-start(s8[6291456]{0:T(1024)(128)(4,1)} %bitcast.322), calls=%async_computation.10 | async-start | bytes 4194304
  498.8 18.2 %copy-start.39 = (bf16[8,1,96,1024]{3,0,2,1:T(8,128)(2,1)S(1)}, bf16[8,1,96,1024]{3,0,2,1:T(8,128)(2,1)}, u32[]{:S(2)}) copy-start(bf16[8,1,96,1024]{3,0,2,1:T(8,128)(2,1)} %reshape.969) | copy-start | bytes 4718596
  521.6 24.4 %copy-start.18 = (bf16[192,16,2,224]{3,0,2,1:T(8,128)(2,1)S(1)}, bf16[192,16,2,224]{3,0,2,1:T(8,128)(2,1)}, u32[]{:S(2)}) copy-start(bf16[192,16,2,224]{3,0,2,1:T(8,128)(2,1)} %copy-done.17) | copy-start | bytes 8257540
  (70 other events, 259.9 us)
Sparse Core Ops, SparseCore 0:
  10.3 52.0 all-gather.7
  64.1 12.6 all-gather.11
  78.4 27.7 all-gather.9
  521.7 92.2 all-reduce.4
where the time goes:
time: 634 us; the launch traced here: 624 us
  matrix products  182 us (29%)
  waiting for transfers between devices  152 us (24%)
  local copies, waits for them, and re-layouts  105 us (17%)
  other arithmetic  78.7 us (12%)
  blocking collectives  66.1 us (10%)
  starting transfers between devices  25.5 us (4%)
  between operations  15.3 us (2%)
    all_to_all x1, waiting for transfers between devices, local(): lax.all_to_all(packed, SP, split_axis=1, concat_axis=0, tiled=True)  61.1 us
    dot_general x6, matrix products, attend_backward(): jnp.einsum('hqk,qhd->khd', p_b, go, preferred_element_type=f32)  51.5 us
    sub x6, other arithmetic, attend_backward(): probs = jax.nn.softmax(scores, axis=-1)  32.6 us
    all_to_all x1, waiting for transfers between devices, local(): lax.all_to_all(grads_heads, SP, split_axis=0, concat_axis=1, tiled=True)  31.9 us
    psum x4, blocking collectives, by_axis(): return functools.reduce(lax.psum, axes, value)  30 us
    psum x1, waiting for transfers between devices, local(): weight_grads = lax.psum(partial_value, SP)  27.2 us
    dot_general x6, matrix products, attend_backward(): jnp.einsum('qhd,khd->hqk', go, values[:end], preferred_element_type=f32)  27.1 us
    dot_general x6, matrix products, attend_backward(): jnp.einsum('hqk,qhd->khd', ds_b, qn, preferred_element_type=f32) * scale  21.1 us
  transfers between devices with their start and end apart: 8, of which 5 were waited for; matrix products, arithmetic and copies ran while one was open for 50% of the time, Pallas kernels for 0%

commit v1 on v0

--- a/solution.py
+++ b/solution.py
@@ -172,7 +172,10 @@
     arrived = lax.all_to_all(packed, SP, split_axis=1, concat_axis=0, tiled=True)
     rope_full = gather_directly(rope_key[0], SP, 0)
     grads_heads, rope_full_grad = attend_backward(arrived, rope_full)
-    returned = lax.all_to_all(grads_heads, SP, split_axis=0, concat_axis=1, tiled=True)
+    returned = jnp.concatenate(
+        lax.all_to_all(jnp.stack(jnp.split(grads_heads, lax.axis_size(SP), axis=0)), SP, 0, 0),
+        axis=1,
+    )
     rope_grad = sent_and_summed(rope_full_grad, SP, 0)
     query_grad = returned[:, :, :width].reshape(tokens, ATTENTION_HEADS * width)
     key_cols = returned[:, :, width : width + PLAIN_HEAD_WIDTH].reshape(tokens, head_cols)

time: 634 us -> 640 us (level)
  local copies, waits for them, and re-layouts: 105 us -> 112 us
    unnamed x173 -> x184, local copies, waits for them, and re-layouts: 10.8 us -> 26 us
    concatenate x1 -> x0, local copies, waits for them, and re-layouts: 8.61 us -> none  [attend_backward(): jnp.concatenate([query_part, dk_nope.astype(bf16), d_vals.astype(bf16)],...]
    another operation x0 -> x2, local copies, waits for them, and re-layouts: none -> 6.79 us  [local(): jnp.stack(jnp.split(grads_heads, lax.axis_size(SP), axis=0))]
  transfers between devices with their start and end apart: 8 -> 8, of which waited for: 5 -> 5; matrix products, arithmetic and copies ran while one was open for 50% -> 51% of each run, Pallas kernels for 0% -> 0%
where the time goes in v1:
time: 640 us; the launch traced here: 630 us
  matrix products  183 us (29%)
  waiting for transfers between devices  150 us (23%)
  local copies, waits for them, and re-layouts  112 us (18%)
  other arithmetic  76.6 us (12%)
  blocking collectives  66.1 us (10%)
  starting transfers between devices  25.9 us (4%)
  between operations  15.3 us (2%)
    all_to_all x1, waiting for transfers between devices, local(): lax.all_to_all(packed, SP, split_axis=1, concat_axis=0, tiled=True)  61.1 us
    dot_general x6, matrix products, attend_backward(): jnp.einsum('hqk,qhd->khd', p_b, go, preferred_element_type=f32)  51.8 us
    sub x6, other arithmetic, attend_backward(): probs = jax.nn.softmax(scores, axis=-1)  32.7 us
    all_to_all x1, waiting for transfers between devices, local(): lax.all_to_all(jnp.stack(jnp.split(grads_heads, lax.axis_size(SP), axis=0...  30.7 us
    psum x4, blocking collectives, by_axis(): return functools.reduce(lax.psum, axes, value)  28.8 us
    psum x1, waiting for transfers between devices, local(): weight_grads = lax.psum(partial_value, SP)  28.2 us
    dot_general x6, matrix products, attend_backward(): jnp.einsum('qhd,khd->hqk', go, values[:end], preferred_element_type=f32)  27.2 us
    unnamed x184, local copies, waits for them, and re-layouts  26 us
  transfers between devices with their start and end apart: 8, of which 5 were waited for; matrix products, arithmetic and copies ran while one was open for 51% of the time, Pallas kernels for 0%

profile of v1, /device:TPU:0, one launch (start us, length us, event | category | flops | bytes accessed | tf_op | source)
XLA Modules:
  0.0 629.6 jit_solution(11218883314387294186)
XLA Ops:
  11.7 15.0 %all-gather.2 = bf16[4,96,1024]{2,1,0:T(8,128)(2,1)} all-gather(bf16[1,96,1024]{2,1,0:T(8,128)(2,1)S(1)} %get-tuple-element.261), channel_id=4, replica_groups=mesh['sp_0'=4,'sp_1'=4,'dp_0'=4,'dp_1'=2] {'dp_0'}, dimensions={0}, use_global_device_ids=true | all-gather | bytes 983040 | tf_op jit(solution)/shard_map/all_gather | solution.py:58
  27.5 8.5 %all-to-all-start.1 = ((bf16[16,192,32]{1,2,0:T(8,128)(2,1)}), bf16[16,192,32]{1,2,0:T(8,128)(2,1)S(1)}, u32[]{:S(2)}, u32[]{:S(2)}) async-start(bf16[16,192,32]{1,2,0:T(8,128)(2,1)} %broadcast_in_dim.80), calls=%async_computation.1 | async-start | bytes 524288 | tf_op jit(solution)/shard_map/all_to_all | solution.py:22
  46.3 16.1 %all-gather.8.cloned.1.call-done = bf16[2,2048,1024]{2,1,0:T(8,128)(2,1)} async-done(((bf16[2,256,1024]{2,1,0:T(8,128)(2,1)}), bf16[2,2048,1024]{2,1,0:T(8,128)(2,1)}) %all-gather.8.cloned.1.call-update) | async-done | bytes 8388624 | tf_op jit(solution)/shard_map/all_gather | solution.py:165
  88.3 7.5 %all-to-all-start = ((bf16[192,32,288]{2,0,1:T(8,128)(2,1)}), bf16[192,32,288]{2,0,1:T(8,128)(2,1)}, u32[]{:S(2)}, u32[]{:S(2)}) async-start(bf16[192,32,288]{2,0,1:T(8,128)(2,1)} %copy.79), calls=%async_computation | async-start | bytes 9437184 | tf_op jit(solution)/shard_map/all_to_all | solution.py:172
  106.3 61.1 %all-to-all-done = bf16[192,32,288]{2,0,1:T(8,128)(2,1)} async-done(((bf16[192,32,288]{2,0,1:T(8,128)(2,1)}), bf16[192,32,288]{2,0,1:T(8,128)(2,1)}, u32[]{:S(2)}, u32[]{:S(2)}) %all-to-all-start) | async-done | bytes 3538976 | tf_op jit(solution)/shard_map/all_to_all | solution.py:172
  167.3 8.3 %copy.80 = bf16[16,192,2,288]{1,0,3,2:T(8,128)(2,1)} copy(bf16[16,192,2,288]{3,1,2,0:T(8,128)(2,1)} %bitcast.8) | data formatting | bytes 7077888 | tf_op jit(solution)/shard_map/all_to_all | solution.py:172
  175.7 7.2 %all_to_all.38 = bf16[3072,2,288]{0,2,1:T(8,128)(2,1)S(1)} reshape(bf16[16,192,2,288]{1,0,3,2:T(8,128)(2,1)} %copy.80) | data formatting | bytes 7077888 | tf_op jit(solution)/shard_map/all_to_all | solution.py:172
  225.7 7.3 %fusion.313 = (f32[2,512]{1,0:T(2,128)S(1)}, f32[2,512,2048]{2,1,0:T(8,128)S(1)}) fusion(f32[2,512,2048]{2,1,0:T(8,128)} %fusion.11), kind=kOutput, calls=%fused_computation.465 | output fusion | flops 4196351 | bytes 16781312 | tf_op jit(solution)/shard_map/sub | solution.py:131
  251.7 6.3 %fusion.314 = (f32[2,512]{1,0:T(2,128)S(1)}, f32[2,512,2560]{2,1,0:T(8,128)}) fusion(f32[2,512,2560]{2,1,0:T(8,128)S(1)} %fusion.9), kind=kOutput, calls=%fused_computation.466 | output fusion | flops 5245439 | bytes 20975616 | tf_op jit(solution)/shard_map/sub | solution.py:131
  283.0 14.9 %fusion.315 = (f32[2,512]{1,0:T(2,128)S(1)}, f32[2,512,3072]{2,1,0:T(8,128)}) fusion(f32[2,512,3072]{2,1,0:T(8,128)} %fusion.7), kind=kOutput, calls=%fused_computation.467 | output fusion | flops 6294527 | bytes 25169920 | tf_op jit(solution)/shard_map/sub | solution.py:131
  297.9 11.8 %multiply_reduce_fusion = (f32[2,512]{1,0:T(2,128)S(1)}, f32[2,512,3072]{2,1,0:T(8,128)}) fusion(f32[2,512,3072]{2,1,0:T(8,128)} %get-tuple-element.301, f32[2,512]{1,0:T(2,128)S(1)} %get-tuple-element.300, bf16[3072,2,288]{0,2,1:T(8,128)(2,1)} %copy-done.6), kind=kOutput, calls=%fused_computation.10 | convolution fusion | flops 412089344 | bytes 26091520 | tf_op jit(solution)/shard_map/qhd,khd->hqk/dot_general | solution.py:132
  309.7 7.2 %multiply_convert_fusion = bf16[2,512,3072]{2,1,0:T(8,128)(2,1)S(1)} fusion(f32[2,512,3072]{2,1,0:T(8,128)} %get-tuple-element.313, f32[2,512]{1,0:T(2,128)S(1)} %get-tuple-element.312, f32[2,512,3072]{2,1,0:T(8,128)S(1)} %bitcast.388, f32[2,512]{1,0:T(2,128)S(1)} %get-tuple-element.300), kind=kLoop, calls=%fused_computation.9 | loop fusion | flops 12582912 | bytes 31465472 | tf_op jit(solution)/shard_map/convert_element_type | solution.py:134
  326.1 6.4 %fusion.99 = f32[3072,2,64]{0,2,1:T(8,128)} fusion(f32[3072,2,64]{0,2,1:T(8,128)} %scatter-add.59, f32[512,2,64]{0,2,1:T(8,128)} %convolution_bitcast_fusion.5, bf16[3072,2,288]{0,2,1:T(8,128)(2,1)} %copy-done.6, f32[2,512]{1,0:T(2,128)S(1)} %get-tuple-element.292, f32[2,512,1024]{2,1,0:T(8,128)} %copy-done.16), kind=kOutput, calls=%fused_computation.121 | convolution fusion | flops 137496576 | bytes 9310208 | tf_op jit(solution)/shard_map/hqk,qhd->khd/dot_general | solution.py:147
  335.4 7.9 %fusion.77 = f32[3072,2,64]{0,2,1:T(8,128)} fusion(f32[3072,2,64]{0,2,1:T(8,128)} %fusion.99, bf16[3072,2,288]{0,2,1:T(8,128)(2,1)} %copy-done.6, f32[2,512]{1,0:T(2,128)S(1)} %get-tuple-element.294, f32[2,512,1536]{2,1,0:T(8,128)} %copy-done.15), kind=kOutput, calls=%fused_computation.91 | convolution fusion | flops 206244352 | bytes 14290944 | tf_op jit(solution)/shard_map/hqk,qhd->khd/dot_general | solution.py:147
  346.2 9.5 %fusion.65 = f32[3072,2,64]{0,2,1:T(8,128)} fusion(f32[3072,2,64]{0,2,1:T(8,128)} %fusion.77, bf16[3072,2,288]{0,2,1:T(8,128)(2,1)} %copy-done.6, f32[2,512]{1,0:T(2,128)S(1)} %get-tuple-element.296, f32[2,512,2048]{2,1,0:T(8,128)} %fusion.11), kind=kOutput, calls=%fused_computation.84 | convolution fusion | flops 274992128 | bytes 19009536 | tf_op jit(solution)/shard_map/hqk,qhd->khd/dot_general | solution.py:147
  360.1 11.6 %fusion.31 = f32[3072,2,64]{0,2,1:T(8,128)} fusion(f32[3072,2,64]{0,2,1:T(8,128)} %fusion.65, bf16[3072,2,288]{0,2,1:T(8,128)(2,1)} %copy-done.6, f32[2,512]{1,0:T(2,128)S(1)} %get-tuple-element.298, f32[2,512,2560]{2,1,0:T(8,128)} %copy-done.3), kind=kOutput, calls=%fused_computation.52 | convolution fusion | flops 343739904 | bytes 23728128 | tf_op jit(solution)/shard_map/hqk,qhd->khd/dot_general | solution.py:147
  376.8 12.7 %fusion.42 = bf16[3072,2,64]{0,2,1:T(8,128)(2,1)} fusion(f32[3072,2,64]{0,2,1:T(8,128)} %fusion.31, bf16[3072,2,288]{0,2,1:T(8,128)(2,1)} %copy-done.6, f32[2,512]{1,0:T(2,128)S(1)} %copy-done.69, f32[2,512,3072]{2,1,0:T(8,128)} %fusion.7), kind=kOutput, calls=%fused_computation.58 | convolution fusion | flops 412880896 | bytes 27660288 | tf_op jit(solution)/shard_map/hqk,qhd->khd/dot_general | solution.py:147
  434.6 30.7 %all-to-all-done.2 = bf16[16,192,2,224]{3,1,2,0:T(8,128)(2,1)} async-done(((bf16[16,192,2,224]{3,1,2,0:T(8,128)(2,1)}), bf16[16,192,2,224]{3,1,2,0:T(8,128)(2,1)}, u32[]{:S(2)}, u32[]{:S(2)}) %all-to-all-start.2) | async-done | bytes 2752544 | tf_op jit(solution)/shard_map/all_to_all | solution.py:176
  506.1 14.2 %all-to-all-done.4 = bf16[1,192,2,2048]{1,2,0,3:T(2,128)(2,1)} async-done(((bf16[1,192,2,2048]{1,2,0,3:T(2,128)(2,1)}), bf16[1,192,2,2048]{1,2,0,3:T(2,128)(2,1)}, u32[]{:S(2)}, u32[]{:S(2)}) %all-to-all-start.4) | async-done | bytes 1572896 | tf_op jit(solution)/shard_map/all_to_all | solution.py:186
  529.9 20.0 %all_to_all.51 = f32[16,192,32]{1,2,0:T(8,128)S(1)} all-to-all(f32[16,192,32]{1,2,0:T(8,128)S(1)} %copy.98), channel_id=1, replica_groups=mesh['sp_0'=4,'sp_1'=4,'dp_0'=4,'dp_1'=2] {'sp_0','sp_1'}, dimensions={0} | all-to-all | bytes 786432 | tf_op jit(solution)/shard_map/all_to_all | solution.py:46
  561.6 8.3 %psum.36 = f32[1024]{0:T(1024)S(1)} all-reduce(f32[1024]{0:T(1024)S(1)} %get-tuple-element.246), channel_id=1, replica_groups=mesh['sp_0'=4,'sp_1'=4,'dp_0'=4,'dp_1'=2] {'sp_0'}, use_global_device_ids=true, to_apply=%region_23.24 | all-reduce | flops 1024 | bytes 8192 | tf_op jit(solution)/shard_map/psum | solution.py:78
  569.9 9.1 %psum.37 = f32[1024]{0:T(1024)S(1)} all-reduce(f32[1024]{0:T(1024)S(1)} %psum.36), channel_id=1, replica_groups=mesh['sp_0'=4,'sp_1'=4,'dp_0'=4,'dp_1'=2] {'sp_1'}, use_global_device_ids=true, to_apply=%region_24.25 | all-reduce | flops 1024 | bytes 8192 | tf_op jit(solution)/shard_map/psum | solution.py:78
  578.9 8.4 %psum.38 = f32[1024]{0:T(1024)S(1)} all-reduce(f32[1024]{0:T(1024)S(1)} %psum.37), channel_id=1, replica_groups=mesh['sp_0'=4,'sp_1'=4,'dp_0'=4,'dp_1'=2] {'dp_0'}, use_global_device_ids=true, to_apply=%region_25.26 | all-reduce | flops 1024 | bytes 8192 | tf_op jit(solution)/shard_map/psum | solution.py:78
  591.5 28.2 %all-reduce.5.cloned.1.call-done = f32[2,256,1024]{2,1,0:T(8,128)} async-done(((f32[2,256,1024]{2,1,0:T(8,128)}), f32[2,256,1024]{2,1,0:T(8,128)}) %all-reduce.5.cloned.1.call-update) | async-done | bytes 2097168 | tf_op jit(solution)/shard_map/psum | solution.py:188
  (330 shorter events, 276.0 us)
Async XLA Ops:
  7.2 19.6 %copy-start.70 = (bf16[1,192,32]{1,2,0:T(8,128)(2,1)S(1)}, bf16[1,192,32]{1,2,0:T(8,128)(2,1)}, u32[]{:S(2)}) copy-start(bf16[1,192,32]{1,2,0:T(8,128)(2,1)} %param.51) | copy-start | bytes 36868
  7.2 55.2 %all-gather.8.cloned.1.call-start = ((), (), s32[]{:S(2)}) async-start(), calls=%async_computation.5 | async-start | bytes 9437184 | tf_op jit(solution)/shard_map/all_gather | solution.py:165
  9.5 29.8 %copy-start.38 = (bf16[1,192,2048]{2,1,0:T(8,128)(2,1)S(1)}, bf16[1,192,2048]{2,1,0:T(8,128)(2,1)}, u32[]{:S(2)}) copy-start(bf16[1,192,2048]{2,1,0:T(8,128)(2,1)} %param.55) | copy-start | bytes 2359300
  9.6 410.0 %all-gather.12.cloned.1.call-start = ((), (), s32[]{:S(2)}) async-start(), calls=%async_computation.8 | async-start | bytes 2359296 | tf_op jit(solution)/shard_map/all_gather | solution.py:58
  10.8 51.6 %copy-start.71 = (f32[192]{0:T(256)}, f32[192]{0:T(256)S(1)}, u32[]{:S(2)}) copy-start(f32[192]{0:T(256)S(1)} %add_rsqrt_fusion) | copy-start | bytes 2308
  27.5 60.8 %all-to-all-start.1 = ((bf16[16,192,32]{1,2,0:T(8,128)(2,1)}), bf16[16,192,32]{1,2,0:T(8,128)(2,1)S(1)}, u32[]{:S(2)}, u32[]{:S(2)}) async-start(bf16[16,192,32]{1,2,0:T(8,128)(2,1)} %broadcast_in_dim.80), calls=%async_computation.1 | async-start | bytes 524288 | tf_op jit(solution)/shard_map/all_to_all | solution.py:22
  36.0 391.5 %all-gather.10.cloned.1.call-start = ((), (), s32[]{:S(2)}) async-start(), calls=%async_computation.7 | async-start | bytes 1966080 | tf_op jit(solution)/shard_map/all_gather | solution.py:58
  39.3 23.1 %copy-start.66 = (f32[1024]{0:T(1024)S(1)}, f32[1024]{0:T(1024)}, u32[]{:S(2)}) copy-start(f32[1024]{0:T(1024)} %param.52) | copy-start | bytes 12292
  88.3 79.0 %all-to-all-start = ((bf16[192,32,288]{2,0,1:T(8,128)(2,1)}), bf16[192,32,288]{2,0,1:T(8,128)(2,1)}, u32[]{:S(2)}, u32[]{:S(2)}) async-start(bf16[192,32,288]{2,0,1:T(8,128)(2,1)} %copy.79), calls=%async_computation | async-start | bytes 9437184 | tf_op jit(solution)/shard_map/all_to_all | solution.py:172
  95.9 8.9 %copy-start.73 = (f32[16]{0:T(128)}, f32[16]{0:T(128)S(1)}, u32[]{:S(2)}) copy-start(f32[16]{0:T(128)S(1)} %negate_power_fusion) | copy-start | bytes 196
  182.8 30.2 %copy-start.6 = (bf16[3072,2,288]{0,2,1:T(8,128)(2,1)}, bf16[3072,2,288]{0,2,1:T(8,128)(2,1)S(1)}, u32[]{:S(2)}) copy-start(bf16[3072,2,288]{0,2,1:T(8,128)(2,1)S(1)} %all_to_all.38) | copy-start | bytes 10616836
  258.8 7.3 %slice-start.7 = ((s8[10485760]{0:T(1024)(128)(4,1)}), s8[2097152]{0:T(1024)(128)(4,1)S(1)}, s32[]{:S(2)}) async-start(s8[10485760]{0:T(1024)(128)(4,1)} %bitcast.389), calls=%async_computation.16 | async-start | bytes 4194304
  297.9 11.8 %copy-start.68 = (f32[2,512]{1,0:T(2,128)}, f32[2,512]{1,0:T(2,128)S(1)}, u32[]{:S(2)}) copy-start(f32[2,512]{1,0:T(2,128)S(1)} %get-tuple-element.300) | copy-start | bytes 12292
  297.9 11.8 %slice-start.2 = ((s8[12582912]{0:T(1024)(128)(4,1)}), s8[4194304]{0:T(1024)(128)(4,1)S(1)}, s32[]{:S(2)}) async-start(s8[12582912]{0:T(1024)(128)(4,1)} %bitcast.387), calls=%async_computation.11 | async-start | bytes 8388608
  297.9 11.8 %slice-start.3 = ((s8[12582912]{0:T(1024)(128)(4,1)}), s8[4194304]{0:T(1024)(128)(4,1)S(1)}, s32[]{:S(2)}) async-start(s8[12582912]{0:T(1024)(128)(4,1)} %bitcast.387), calls=%async_computation.12 | async-start | bytes 8388608
  297.9 11.8 %slice-start.4 = ((s8[12582912]{0:T(1024)(128)(4,1)}), s8[4194304]{0:T(1024)(128)(4,1)S(1)}, s32[]{:S(2)}) async-start(s8[12582912]{0:T(1024)(128)(4,1)} %bitcast.387), calls=%async_computation.13 | async-start | bytes 8388608
  414.2 51.1 %all-to-all-start.2 = ((bf16[16,192,2,224]{3,1,2,0:T(8,128)(2,1)}), bf16[16,192,2,224]{3,1,2,0:T(8,128)(2,1)}, u32[]{:S(2)}, u32[]{:S(2)}) async-start(bf16[16,192,2,224]{3,1,2,0:T(8,128)(2,1)} %copy.91), calls=%async_computation.2 | async-start | bytes 6291456 | tf_op jit(solution)/shard_map/all_to_all | solution.py:176
  423.8 7.3 %copy-start.10 = (bf16[3072,2,16]{0,2,1:T(8,128)(2,1)S(1)}, bf16[3072,2,16]{0,2,1:T(8,128)(2,1)}, u32[]{:S(2)}) copy-start(bf16[3072,2,16]{0,2,1:T(8,128)(2,1)} %copy-done.8) | copy-start | bytes 589828
  423.8 7.3 %copy-start.13 = (bf16[3072,2,16]{0,2,1:T(8,128)(2,1)S(1)}, bf16[3072,2,16]{0,2,1:T(8,128)(2,1)}, u32[]{:S(2)}) copy-start(bf16[3072,2,16]{0,2,1:T(8,128)(2,1)} %copy-done.11) | copy-start | bytes 589828
  488.7 31.5 %all-to-all-start.4 = ((bf16[1,192,2,2048]{1,2,0,3:T(2,128)(2,1)}), bf16[1,192,2,2048]{1,2,0,3:T(2,128)(2,1)}, u32[]{:S(2)}, u32[]{:S(2)}) async-start(bf16[1,192,2,2048]{1,2,0,3:T(2,128)(2,1)} %copy.99), calls=%async_computation.4 | async-start | bytes 4194304 | tf_op jit(solution)/shard_map/all_to_all | solution.py:186
  493.1 126.7 %all-reduce.5.cloned.1.call-start = ((), (), s32[]{:S(2)}) async-start(), calls=%async_computation.6 | async-start | bytes 4194304 | tf_op jit(solution)/shard_map/psum | solution.py:188
  493.1 10.6 %slice-start = ((s8[6291456]{0:T(1024)(128)(4,1)}), s8[4194304]{0:T(1024)(128)(4,1)S(1)}, s32[]{:S(2)}) async-start(s8[6291456]{0:T(1024)(128)(4,1)} %bitcast.385), calls=%async_computation.9 | async-start | bytes 8388608
  495.5 8.2 %slice-start.1 = ((s8[6291456]{0:T(1024)(128)(4,1)}), s8[2097152]{0:T(1024)(128)(4,1)S(1)}, s32[]{:S(2)}) async-start(s8[6291456]{0:T(1024)(128)(4,1)} %bitcast.385), calls=%async_computation.10 | async-start | bytes 4194304
  503.7 20.2 %copy-start.36 = (bf16[8,1,96,1024]{3,0,2,1:T(8,128)(2,1)S(1)}, bf16[8,1,96,1024]{3,0,2,1:T(8,128)(2,1)}, u32[]{:S(2)}) copy-start(bf16[8,1,96,1024]{3,0,2,1:T(8,128)(2,1)} %reshape.977) | copy-start | bytes 4718596
  (67 other events, 254.8 us)
Sparse Core Ops, SparseCore 0:
  10.3 52.0 all-gather.7
  64.0 12.7 all-gather.11
  78.6 27.7 all-gather.9
  528.6 91.0 all-reduce.4
